TPU v7x, 32 devices: a whole 2x2x4 slice. The times are simulated.
32 devices in a mesh: rep: 4 (over z), fs: 2 (over y), tp: 4 (over x, core).
Axes of the slice: x: 2, y: 2, z: 4, core: 2. Of those that a mesh axis runs over, the one named last changes fastest.
Arguments:
- tokens: bfloat16 [3072, 2048], P('rep', 'fs'), may hold values from -6 to 6
- gate_pre: bfloat16 [3072, 6144], P('rep', 'tp'), may hold values from -6 to 6
- up_pre: bfloat16 [3072, 6144], P('rep', 'tp'), may hold values from -6 to 6
- hidden_grad: bfloat16 [3072, 6144], P('rep', 'tp'), may hold values from -0.75 to 0.75
- gate_weight: bfloat16 [2048, 6144], P('fs', 'tp'), may hold values from -0.125 to 0.125
- up_weight: bfloat16 [2048, 6144], P('fs', 'tp'), may hold values from -0.125 to 0.125
- gate_taps: float32 [3, 6144], P(None, 'tp'), may hold values from -3.5 to 3.5
- up_taps: float32 [3, 6144], P(None, 'tp'), may hold values from -3.5 to 3.5
- gate_bias: float32 [6144], P('tp'), may hold values from -4 to 4
- up_bias: float32 [6144], P('tp'), may hold values from -4 to 4
Outputs:
- input_grad: bfloat16 [3072, 2048], P('rep', 'fs')
- gate_weight_grad: float32 [2048, 6144], P('fs', 'tp')
- up_weight_grad: float32 [2048, 6144], P('fs', 'tp')
- gate_taps_grad: float32 [3, 6144], P(None, 'tp')
- up_taps_grad: float32 [3, 6144], P(None, 'tp')
- gate_bias_grad: float32 [6144], P('tp')
- up_bias_grad: float32 [6144], P('tp')
All inputs are finite; a program needn't handle non-finite values.
Results may differ from a plain program's by a relative error of at most 0.017.
Values may be sent and summed in bfloat16 or wider, within the bound.
A program may use at most 64 MiB of HBM per device.

v0:
```python
import jax
import jax.numpy as jnp
from jax import lax
from jax.sharding import PartitionSpec as P


def causal_mix(signal, tap_weights):
    tap_count = tap_weights.shape[0]
    length = signal.shape[0]
    padded = jnp.pad(signal, ((tap_count - 1, 0), (0, 0)))
    mixed = padded[0:length] * tap_weights[0]
    for offset in range(1, tap_count):
        mixed = mixed + padded[offset : offset + length] * tap_weights[offset]
    return mixed


def mix_back(signal, tap_weights):
    tap_count = tap_weights.shape[0]
    length = signal.shape[0]
    padded = jnp.pad(signal, ((0, tap_count - 1), (0, 0)))
    begin = tap_count - 1
    mixed = padded[begin : begin + length] * tap_weights[0]
    for offset in range(1, tap_count):
        begin = tap_count - 1 - offset
        mixed = mixed + padded[begin : begin + length] * tap_weights[offset]
    return mixed


def tap_terms(grad_signal, signal, tap_count):
    length = signal.shape[0]
    padded = jnp.pad(signal, ((tap_count - 1, 0), (0, 0)))
    return jnp.stack(
        [
            jnp.sum(grad_signal * padded[offset : offset + length], axis=0)
            for offset in range(tap_count)
        ]
    )


def backward_terms(gate_pre, up_pre, hidden_grad, gate_taps, up_taps, gate_bias, up_bias):
    gate_float = gate_pre.astype(jnp.float32)
    up_float = up_pre.astype(jnp.float32)
    gate_mixed = causal_mix(gate_float, gate_taps) + gate_bias
    up_mixed = causal_mix(up_float, up_taps) + up_bias
    logistic = jax.nn.sigmoid(gate_mixed)
    cotangent = hidden_grad.astype(jnp.float32)
    gate_delta = cotangent * up_mixed * logistic * (1.0 + gate_mixed * (1.0 - logistic))
    up_delta = cotangent * gate_mixed * logistic
    gate_back = mix_back(gate_delta, gate_taps).astype(jnp.bfloat16)
    up_back = mix_back(up_delta, up_taps).astype(jnp.bfloat16)
    tap_count = gate_taps.shape[0]
    return (
        gate_back,
        up_back,
        tap_terms(gate_delta, gate_float, tap_count),
        tap_terms(up_delta, up_float, tap_count),
        jnp.sum(gate_delta, axis=0),
        jnp.sum(up_delta, axis=0),
    )


def per_device(
    tokens,
    gate_pre,
    up_pre,
    hidden_grad,
    gate_weight,
    up_weight,
    gate_taps,
    up_taps,
    gate_bias,
    up_bias,
):
    gate_back, up_back, gate_tap_part, up_tap_part, gate_bias_part, up_bias_part = backward_terms(
        gate_pre, up_pre, hidden_grad, gate_taps, up_taps, gate_bias, up_bias
    )
    feature_dims = (((1,), (1,)), ((), ()))
    token_dims = (((0,), (0,)), ((), ()))
    full_partial = lax.dot_general(
        gate_back, gate_weight, feature_dims, preferred_element_type=jnp.float32
    ) + lax.dot_general(up_back, up_weight, feature_dims, preferred_element_type=jnp.float32)
    own_columns = lax.psum_scatter(
        full_partial.astype(jnp.bfloat16), "tp", scatter_dimension=1, tiled=True
    )
    result = lax.all_gather(own_columns, "tp", axis=1, tiled=True)
    gate_local = lax.dot_general(tokens, gate_back, token_dims, preferred_element_type=jnp.float32)
    up_local = lax.dot_general(tokens, up_back, token_dims, preferred_element_type=jnp.float32)
    summed_grads = (
        lax.psum(gate_local.astype(jnp.bfloat16), "rep").astype(jnp.float32),
        lax.psum(up_local.astype(jnp.bfloat16), "rep").astype(jnp.float32),
        lax.psum(gate_tap_part.astype(jnp.bfloat16), "rep").astype(jnp.float32),
        lax.psum(up_tap_part.astype(jnp.bfloat16), "rep").astype(jnp.float32),
        lax.psum(gate_bias_part.astype(jnp.bfloat16), "rep").astype(jnp.float32),
        lax.psum(up_bias_part.astype(jnp.bfloat16), "rep").astype(jnp.float32),
    )
    gate_weight_grad, up_weight_grad, gate_taps_grad, up_taps_grad, gate_bias_grad, up_bias_grad = (
        summed_grads
    )
    return (
        result,
        gate_weight_grad,
        up_weight_grad,
        gate_taps_grad,
        up_taps_grad,
        gate_bias_grad,
        up_bias_grad,
    )


def solution(mesh):
    return jax.shard_map(
        per_device,
        mesh=mesh,
        in_specs=(
            P("rep", "fs"),
            P("rep", "tp"),
            P("rep", "tp"),
            P("rep", "tp"),
            P("fs", "tp"),
            P("fs", "tp"),
            P(None, "tp"),
            P(None, "tp"),
            P("tp"),
            P("tp"),
        ),
        out_specs=(
            P("rep", "fs"),
            P("fs", "tp"),
            P("fs", "tp"),
            P(None, "tp"),
            P(None, "tp"),
            P("tp"),
            P("tp"),
        ),
        check_vma=False,
    )
```

profile of v0, /device:TPU:0, one launch (start us, length us, event | category | flops | bytes accessed | tf_op | source)
XLA Modules:
  0.0 329.4 jit_solution(4718363927047613101)
XLA Ops:
  8.0 0.0 copy-start
  8.0 0.0 reduce-scatter.2.cloned.1.call-start
  8.1 0.0 copy-start.3
  8.1 1.0 slice_reduce_fusion.2
  9.1 1.0 slice_reduce_fusion.5
  10.0 2.3 convert_element_type.66
  12.3 0.0 copy-done.3
  12.4 0.0 copy-start.2
  12.4 0.0 copy-start.7
  12.4 0.6 convert_element_type.65
  13.0 1.0 copy-done.2
  14.0 0.0 copy-done.7
  14.0 5.8 %fusion.5 = (bf16[1536]{0:T(1024)(128)(2,1)S(1)}, bf16[1536]{0:T(1024)(128)(2,1)S(1)}, bf16[1536]{0:T(1024)(128)(2,1)S(1)}, bf16[1536]{0:T(1024)(128)(2,1)S(1)},...) fusion(bf16[768,1536]{1,0:T(8,128)(2,1)S(1)} %copy-done.3, f32[768,1536]{1,0:T(8,128)S(1)} %convert_element_type.65, ...), kind=kLoop, calls=%fused_computation.32 | loop fusion | flops 23586816 | bytes 23629824 | tf_op jit(solution)/shard_map/reduce_sum | solution.py:58
  19.8 0.0 copy-done.8
  19.8 10.3 %fusion.6 = (bf16[1536]{0:T(1024)(128)(2,1)S(1)}, bf16[1536]{0:T(1024)(128)(2,1)S(1)}, bf16[1536]{0:T(1024)(128)(2,1)S(1)}, bf16[1536]{0:T(1024)(128)(2,1)S(1)},...) fusion(bf16[768,1536]{1,0:T(8,128)(2,1)} %param.11, f32[768,1536]{1,0:T(8,128)S(1)} %convert_element_type.66, ...), kind=kLoop, calls=%fused_computation.33 | loop fusion | flops 35383296 | bytes 30707712 | tf_op jit(solution)/shard_map/reduce_sum | solution.py:57
  30.1 5.9 %add_convert_fusion.1 = bf16[768,1536]{1,0:T(8,128)(2,1)S(1)} fusion(f32[768,1536]{1,0:T(8,128)} %get-tuple-element.40, f32[1536]{0:T(1024)S(1)} %get-tuple-element.30, f32[1536]{0:T(1024)S(1)} %get-tuple-element.31, f32[1536]{0:T(1024)S(1)} %get-tuple-element.29), kind=kLoop, calls=%fused_computation.12 | loop fusion | flops 7077888 | bytes 7096320 | tf_op jit(solution)/shard_map/convert_element_type | solution.py:49
  36.1 0.0 copy-done
  36.1 0.0 copy-start.6
  36.1 0.0 copy-start.4
  36.1 0.0 copy-start.9
  36.1 2.6 fusion.9
  38.7 0.0 copy-done.6
  38.7 0.0 copy-done.4
  38.8 0.8 copy-done.9
  39.5 3.7 %add_convert_fusion.2 = bf16[768,1024]{1,0:T(8,128)(2,1)} fusion(f32[768,1024]{1,0:T(8,128)S(1)} %fusion.9, bf16[768,1536]{1,0:T(8,128)(2,1)S(1)} %copy-done.4, bf16[1024,1536]{1,0:T(8,128)(2,1)S(1)} %copy-done.9), kind=kOutput, calls=%fused_computation.23 | convolution fusion | flops 2417491968 | bytes 10223616 | tf_op jit(solution)/shard_map/dot_general | solution.py:81
  43.2 0.0 reduce-scatter.2.cloned.1.call-update
  43.3 0.0 all-gather.2.cloned.1.call-start
  43.3 30.9 %reduce-scatter.2.cloned.1.call-done = bf16[768,256]{1,0:T(8,128)(2,1)} async-done(((bf16[768,1024]{1,0:T(8,128)(2,1)}), bf16[768,256]{1,0:T(8,128)(2,1)}) %reduce-scatter.2.cloned.1.call-update) | async-done | bytes 393232 | tf_op jit(solution)/shard_map/reduce_scatter | solution.py:82
  74.2 0.0 all-gather.2.cloned.1.call-update
  74.2 0.0 copy-start.5
  74.2 0.0 all-reduce.8.cloned.1.call-start
  74.3 0.0 copy-start.10
  74.3 6.6 %fusion.3 = bf16[1024,1536]{0,1:T(8,128)(2,1)} fusion(bf16[768,1536]{1,0:T(8,128)(2,1)} %copy-done.6, bf16[768,1024]{1,0:T(8,128)(2,1)} %param.10), kind=kOutput, calls=%fused_computation.21 | convolution fusion | flops 2417491968 | bytes 7077888 | tf_op jit(solution)/shard_map/dot_general | solution.py:86
  80.9 0.0 copy-done.5
  80.9 0.0 copy-done.10
  80.9 4.0 %fusion.4 = bf16[1024,1536]{0,1:T(8,128)(2,1)} fusion(bf16[768,1536]{1,0:T(8,128)(2,1)S(1)} %copy-done.5, bf16[768,1024]{1,0:T(8,128)(2,1)S(1)} %copy-done.10), kind=kOutput, calls=%fused_computation.22 | convolution fusion | flops 2417491968 | bytes 7077888 | tf_op jit(solution)/shard_map/dot_general | solution.py:87
  84.9 0.0 all-reduce.8.cloned.1.call-update
  85.0 0.1 pad_maximum_fusion
  85.1 21.1 %all-reduce.4 = (bf16[3,1536]{1,0:T(4,128)(2,1)S(1)}, bf16[3,1536]{1,0:T(4,128)(2,1)S(1)}, bf16[1536]{0:T(1024)(128)(2,1)S(1)}, bf16[1536]{0:T(1024)(128)(2,1)S(1)}) all-reduce(bf16[3,1536]{1,0:T(4,128)(2,1)S(1)} %get-tuple-element.42, bf16[3,1536]{1,0:T(4,128)(2,1)S(1)} %get-tuple-element.43, ...), channel_id=1, replica_groups=mesh['rep'=4,'fs'=2,'tp'=4] {'rep'}, use_global_device_ids=true, to_apply=%region_6.7 | all-reduce | flops 12288 | bytes 49152 | tf_op jit(solution)/shard_map/psum | solution.py:91
  106.2 0.6 convert_element_type.79
  106.8 0.6 convert_element_type.81
  107.4 0.6 convert_element_type.76
  108.0 0.6 convert_element_type.77
  108.6 199.7 %all-reduce.8.cloned.1.call-done = (bf16[1024,1536]{0,1:T(8,128)(2,1)}, bf16[1024,1536]{0,1:T(8,128)(2,1)}) async-done(((bf16[1024,1536]{0,1:T(8,128)(2,1)}, bf16[1024,1536]{0,1:T(8,128)(2,1)}), (bf16[1024,1536]{0,1:T(8,128)(2,1)}, bf16[1024,1536]{0,1:T(8,128)(2,1)})) %all-reduce.8.cloned.1.call-update) | async-done | bytes 6291472 | tf_op jit(solution)/shard_map/psum | solution.py:89
  308.3 5.4 %copy.17 = f32[1024,1536]{1,0:T(8,128)} copy(bf16[1024,1536]{0,1:T(8,128)(2,1)} %get-tuple-element.36) | data formatting | bytes 9437184
  313.7 5.5 %copy.18 = f32[1024,1536]{1,0:T(8,128)} copy(bf16[1024,1536]{0,1:T(8,128)(2,1)} %get-tuple-element.37) | data formatting | bytes 9437184
  319.2 2.7 copy.22
  321.9 0.0 copy-done.1
  (9 shorter events, 0.0 us)
Async XLA Ops:
  8.0 28.1 %copy-start = (bf16[1024,1536]{1,0:T(8,128)(2,1)S(1)}, bf16[1024,1536]{1,0:T(8,128)(2,1)}, u32[]{:S(2)}) copy-start(bf16[1024,1536]{1,0:T(8,128)(2,1)} %param.14) | copy-start | bytes 9437188
  8.0 66.2 %reduce-scatter.2.cloned.1.call-start = ((), (), s32[]{:S(2)}) async-start(), calls=%async_computation.1 | async-start | bytes 1966080 | tf_op jit(solution)/shard_map/reduce_scatter | solution.py:82
  8.1 4.3 %copy-start.3 = (bf16[768,1536]{1,0:T(8,128)(2,1)S(1)}, bf16[768,1536]{1,0:T(8,128)(2,1)}, u32[]{:S(2)}) copy-start(bf16[768,1536]{1,0:T(8,128)(2,1)} %param.12) | copy-start | bytes 7077892
  12.4 1.7 copy-start.2
  12.4 1.7 copy-start.7
  14.0 5.8 %copy-start.8 = (f32[1536]{0:T(1024)S(1)}, f32[1536]{0:T(1024)}, u32[]{:S(2)}) copy-start(f32[1536]{0:T(1024)} %param.19) | copy-start | bytes 18436
  36.1 2.7 copy-start.6
  36.1 2.7 copy-start.4
  36.1 3.4 %copy-start.9 = (bf16[1024,1536]{1,0:T(8,128)(2,1)S(1)}, bf16[1024,1536]{1,0:T(8,128)(2,1)}, u32[]{:S(2)}) copy-start(bf16[1024,1536]{1,0:T(8,128)(2,1)} %param.15) | copy-start | bytes 9437188
  43.3 65.4 %all-gather.2.cloned.1.call-start = ((), (), s32[]{:S(2)}) async-start(), calls=%async_computation.2 | async-start | bytes 1966080 | tf_op jit(solution)/shard_map/all_gather | solution.py:85
  74.2 6.7 %copy-start.5 = (bf16[768,1536]{1,0:T(8,128)(2,1)S(1)}, bf16[768,1536]{1,0:T(8,128)(2,1)}, u32[]{:S(2)}) copy-start(bf16[768,1536]{1,0:T(8,128)(2,1)} %get-tuple-element.41) | copy-start | bytes 7077892
  74.2 234.1 %all-reduce.8.cloned.1.call-start = ((), (), s32[]{:S(2)}) async-start(), calls=%async_computation.3 | async-start | bytes 12582912 | tf_op jit(solution)/shard_map/psum | solution.py:89
  74.3 6.6 %copy-start.10 = (bf16[768,1024]{1,0:T(8,128)(2,1)S(1)}, bf16[768,1024]{1,0:T(8,128)(2,1)}, u32[]{:S(2)}) copy-start(bf16[768,1024]{1,0:T(8,128)(2,1)} %param.10) | copy-start | bytes 4718596
  313.7 8.2 %copy-start.1 = (bf16[1024,1536]{1,0:T(8,128)(2,1)S(1)}, bf16[1024,1536]{1,0:T(8,128)(2,1)}, u32[]{:S(2)}) copy-start(bf16[1024,1536]{1,0:T(8,128)(2,1)} %param.14) | copy-start | bytes 9437188
Sparse Core Ops, SparseCore 0:
  43.4 30.7 reduce-scatter.1
  75.7 19.8 all-gather.1
Sparse Core Ops, SparseCore 1:
  85.0 223.3 all-reduce.7
where the time goes:
time: 330 us; the launch traced here: 329 us
  waiting for transfers between devices  231 us (70%)
  other arithmetic  27.4 us (8%)
  blocking collectives  21.1 us (6%)
  local copies, waits for them, and re-layouts  17.4 us (5%)
  matrix products  17 us (5%)
  between operations  15.7 us (5%)
    psum x1, waiting for transfers between devices, per_device(): lax.psum(gate_local.astype(jnp.bfloat16), 'rep').astype(jnp.float32)  200 us
    reduce_scatter x1, waiting for transfers between devices, per_device(): lax.psum_scatter(full_partial.astype(jnp.bfloat16), 'tp', scatter_dimensi...  30.9 us
    psum x1, blocking collectives, per_device(): lax.psum(gate_tap_part.astype(jnp.bfloat16), 'rep').astype(jnp.float32)  21.1 us
    unnamed x25, local copies, waits for them, and re-layouts  15.4 us
    reduce_sum x1, other arithmetic, backward_terms(): jnp.sum(gate_delta, axis=0)  10.3 us
  transfers between devices with their start and end apart: 3, of which 2 were waited for; matrix products, arithmetic and copies ran while one was open for 4% of the time, Pallas kernels for 0%

commit v1 on v0

--- a/solution.py
+++ b/solution.py
@@ -86,7 +86,7 @@
     gate_local = lax.dot_general(tokens, gate_back, token_dims, preferred_element_type=jnp.float32)
     up_local = lax.dot_general(tokens, up_back, token_dims, preferred_element_type=jnp.float32)
     summed_grads = (
-        lax.psum(gate_local.astype(jnp.bfloat16), "rep").astype(jnp.float32),
+        jnp.sum(lax.all_gather(gate_local.astype(jnp.bfloat16), "rep"), axis=0).astype(jnp.float32),
         lax.psum(up_local.astype(jnp.bfloat16), "rep").astype(jnp.float32),
         lax.psum(gate_tap_part.astype(jnp.bfloat16), "rep").astype(jnp.float32),
         lax.psum(up_tap_part.astype(jnp.bfloat16), "rep").astype(jnp.float32),

time: 330 us -> 427 us (1.29)
  waiting for transfers between devices: 231 us -> 288 us
  local copies, waits for them, and re-layouts: 17.4 us -> 36.6 us
  other arithmetic: 27.4 us -> 46.2 us
    psum x1, waiting for transfers between devices: 200 us -> 263 us  [per_device(): lax.psum(up_local.astype(jnp.bfloat16), 'rep').astype(jnp.float32)]
    all_gather x0 -> x1, local copies, waits for them, and re-layouts: none -> 21.2 us  [per_device(): lax.all_gather(gate_local.astype(jnp.bfloat16), 'rep')]
    reduce_sum x0 -> x1, other arithmetic: none -> 18.6 us  [per_device(): jnp.sum(lax.all_gather(gate_local.astype(jnp.bfloat16), 'rep'), axis=0)]
    reduce_scatter x1, waiting for transfers between devices: 30.9 us -> 25.3 us  [per_device(): lax.psum_scatter(full_partial.astype(jnp.bfloat16), 'tp', scatter_dimensi...]
    unnamed x25 -> x27, local copies, waits for them, and re-layouts: 15.4 us -> 15.2 us
  transfers between devices with their start and end apart: 3 -> 4, of which waited for: 2 -> 2; matrix products, arithmetic and copies ran while one was open for 4% -> 5% of each run, Pallas kernels for 0% -> 0%
where the time goes in v1:
time: 427 us; the launch traced here: 426 us
  waiting for transfers between devices  288 us (67%)
  other arithmetic  46.2 us (11%)
  local copies, waits for them, and re-layouts  36.6 us (9%)
  blocking collectives  20.5 us (5%)
  matrix products  18.2 us (4%)
  between operations  15.4 us (4%)
    psum x1, waiting for transfers between devices, per_device(): lax.psum(up_local.astype(jnp.bfloat16), 'rep').astype(jnp.float32)  263 us
    reduce_scatter x1, waiting for transfers between devices, per_device(): lax.psum_scatter(full_partial.astype(jnp.bfloat16), 'tp', scatter_dimensi...  25.3 us
    all_gather x1, local copies, waits for them, and re-layouts, per_device(): lax.all_gather(gate_local.astype(jnp.bfloat16), 'rep')  21.2 us
    psum x1, blocking collectives, per_device(): lax.psum(gate_tap_part.astype(jnp.bfloat16), 'rep').astype(jnp.float32)  20.5 us
    reduce_sum x1, other arithmetic, per_device(): jnp.sum(lax.all_gather(gate_local.astype(jnp.bfloat16), 'rep'), axis=0)  18.6 us
    unnamed x27, local copies, waits for them, and re-layouts  15.2 us
    reduce_sum x1, other arithmetic, backward_terms(): jnp.sum(gate_delta, axis=0)  10.3 us
  transfers between devices with their start and end apart: 4, of which 2 were waited for; matrix products, arithmetic and copies ran while one was open for 5% of the time, Pallas kernels for 0%

profile of v1, /device:TPU:0, one launch (start us, length us, event | category | flops | bytes accessed | tf_op | source)
XLA Modules:
  0.0 425.6 jit_solution(3481755478058599422)
XLA Ops:
  8.0 0.0 copy-start
  8.0 0.0 reduce-scatter.2.cloned.1.call-start
  8.1 0.0 copy-start.3
  8.1 2.5 convert_element_type.68
  10.5 0.0 copy-done.3
  10.6 0.6 convert_element_type.67
  11.2 0.1 copy-done.7
  11.3 0.1 slice_reduce_fusion.2
  11.4 0.0 copy-done.8
  11.4 0.1 slice_reduce_fusion.5
  11.4 0.8 copy-done.2
  12.3 0.0 copy-done.9
  12.3 5.8 %fusion.5 = (bf16[1536]{0:T(1024)(128)(2,1)S(1)}, bf16[1536]{0:T(1024)(128)(2,1)S(1)}, bf16[1536]{0:T(1024)(128)(2,1)S(1)}, bf16[1536]{0:T(1024)(128)(2,1)S(1)},...) fusion(bf16[768,1536]{1,0:T(8,128)(2,1)S(1)} %copy-done.3, f32[768,1536]{1,0:T(8,128)S(1)} %convert_element_type.67, ...), kind=kLoop, calls=%fused_computation.32 | loop fusion | flops 23586816 | bytes 23629824 | tf_op jit(solution)/shard_map/reduce_sum | solution.py:58
  18.0 0.0 copy-done.10
  18.1 10.3 %fusion.6 = (bf16[1536]{0:T(1024)(128)(2,1)S(1)}, bf16[1536]{0:T(1024)(128)(2,1)S(1)}, bf16[1536]{0:T(1024)(128)(2,1)S(1)}, bf16[1536]{0:T(1024)(128)(2,1)S(1)},...) fusion(bf16[768,1536]{1,0:T(8,128)(2,1)} %param.11, f32[768,1536]{1,0:T(8,128)S(1)} %convert_element_type.68, ...), kind=kLoop, calls=%fused_computation.33 | loop fusion | flops 35383296 | bytes 30707712 | tf_op jit(solution)/shard_map/reduce_sum | solution.py:57
  28.4 6.0 %add_convert_fusion.1 = bf16[768,1536]{1,0:T(8,128)(2,1)S(1)} fusion(f32[768,1536]{1,0:T(8,128)} %get-tuple-element.45, f32[1536]{0:T(1024)S(1)} %get-tuple-element.37, f32[1536]{0:T(1024)S(1)} %get-tuple-element.38, f32[1536]{0:T(1024)S(1)} %get-tuple-element.36), kind=kLoop, calls=%fused_computation.12 | loop fusion | flops 7077888 | bytes 7096320 | tf_op jit(solution)/shard_map/convert_element_type | solution.py:49
  34.4 0.0 copy-done
  34.4 0.0 copy-start.6
  34.4 0.0 copy-start.4
  34.4 0.0 copy-start.11
  34.4 2.6 fusion.9
  37.1 0.0 copy-done.6
  37.1 0.0 copy-done.4
  37.1 0.8 copy-done.11
  37.9 3.7 add_convert_fusion.2
  41.6 0.0 reduce-scatter.2.cloned.1.call-update
  41.6 0.0 all-reduce.7.cloned.1.call-start
  41.7 0.0 copy-done.5
  41.7 5.5 %fusion.4 = bf16[1024,1536]{0,1:T(8,128)(2,1)} fusion(bf16[768,1536]{1,0:T(8,128)(2,1)S(1)} %copy-done.5, bf16[768,1024]{1,0:T(8,128)(2,1)} %param.10), kind=kOutput, calls=%fused_computation.22 | convolution fusion | flops 2417491968 | bytes 7077888 | tf_op jit(solution)/shard_map/dot_general | solution.py:87
  47.1 0.0 all-reduce.7.cloned.1.call-update
  47.1 0.0 all-gather.4.cloned.1.call-start
  47.2 25.3 %reduce-scatter.2.cloned.1.call-done = bf16[768,256]{1,0:T(8,128)(2,1)} async-done(((bf16[768,1024]{1,0:T(8,128)(2,1)}), bf16[768,256]{1,0:T(8,128)(2,1)}) %reduce-scatter.2.cloned.1.call-update) | async-done | bytes 393232 | tf_op jit(solution)/shard_map/reduce_scatter | solution.py:82
  72.5 0.0 all-gather.4.cloned.1.call-update
  72.6 0.2 all-gather.6.cloned.1.call-start
  72.8 6.4 %fusion.3 = bf16[1024,1536]{0,1:T(8,128)(2,1)} fusion(bf16[768,1536]{1,0:T(8,128)(2,1)} %copy-done.6, bf16[768,1024]{1,0:T(8,128)(2,1)} %param.10), kind=kOutput, calls=%fused_computation.21 | convolution fusion | flops 2417491968 | bytes 7077888 | tf_op jit(solution)/shard_map/dot_general | solution.py:86
  79.2 0.0 all-gather.6.cloned.1.call-update
  79.3 0.1 pad_maximum_fusion
  79.4 20.5 %all-reduce.4 = (bf16[3,1536]{1,0:T(4,128)(2,1)S(1)}, bf16[3,1536]{1,0:T(4,128)(2,1)S(1)}, bf16[1536]{0:T(1024)(128)(2,1)S(1)}, bf16[1536]{0:T(1024)(128)(2,1)S(1)}) all-reduce(bf16[3,1536]{1,0:T(4,128)(2,1)S(1)} %get-tuple-element.47, bf16[3,1536]{1,0:T(4,128)(2,1)S(1)} %get-tuple-element.48, ...), channel_id=1, replica_groups=mesh['rep'=4,'fs'=2,'tp'=4] {'rep'}, use_global_device_ids=true, to_apply=%region_6.7 | all-reduce | flops 12288 | bytes 49152 | tf_op jit(solution)/shard_map/psum | solution.py:91
  99.9 0.6 convert_element_type.78
  100.5 0.6 convert_element_type.79
  101.1 0.6 convert_element_type.81
  101.7 0.6 convert_element_type.83
  102.3 262.8 %all-reduce.7.cloned.1.call-done = bf16[1024,1536]{0,1:T(8,128)(2,1)} async-done(((bf16[1024,1536]{0,1:T(8,128)(2,1)}), bf16[1024,1536]{0,1:T(8,128)(2,1)}) %all-reduce.7.cloned.1.call-update) | async-done | bytes 3145744 | tf_op jit(solution)/shard_map/psum | solution.py:90
  365.2 5.4 %copy.19 = f32[1024,1536]{1,0:T(8,128)} copy(bf16[1024,1536]{0,1:T(8,128)(2,1)} %all-reduce.7.cloned.1.call-done) | data formatting | bytes 9437184
  370.6 21.2 %reshape.16 = bf16[4,1024,1536]{1,0,2:T(4,128)(2,1)} reshape(bf16[4096,1536]{0,1:T(8,128)(2,1)} %all-gather.6.cloned.1.call-done) | data formatting | bytes 25165824 | tf_op jit(solution)/shard_map/all_gather | solution.py:89
  391.8 18.6 %reduce_sum.84 = bf16[1024,1536]{0,1:T(8,128)(2,1)} reduce(bf16[4,1024,1536]{1,0,2:T(4,128)(2,1)} %reshape.16, bf16[]{:T(256)} %constant.7.clone.1), dimensions={0}, to_apply=%region_1.2 | reduce | flops 4718592 | bytes 15728642 | tf_op jit(solution)/shard_map/reduce_sum | solution.py:89
  410.4 5.4 %copy.18 = f32[1024,1536]{1,0:T(8,128)} copy(bf16[1024,1536]{0,1:T(8,128)(2,1)} %reduce_sum.84) | data formatting | bytes 9437184
  415.8 2.7 copy.22
  (16 shorter events, 0.1 us)
Async XLA Ops:
  8.0 26.4 %copy-start = (bf16[1024,1536]{1,0:T(8,128)(2,1)S(1)}, bf16[1024,1536]{1,0:T(8,128)(2,1)}, u32[]{:S(2)}) copy-start(bf16[1024,1536]{1,0:T(8,128)(2,1)} %param.14) | copy-start | bytes 9437188
  8.0 64.5 %reduce-scatter.2.cloned.1.call-start = ((), (), s32[]{:S(2)}) async-start(), calls=%async_computation.1 | async-start | bytes 1966080 | tf_op jit(solution)/shard_map/reduce_scatter | solution.py:82
  8.1 2.5 copy-start.3
  10.6 0.7 copy-start.7
  10.6 0.8 copy-start.8
  10.6 1.7 copy-start.2
  10.6 1.7 copy-start.9
  12.3 5.8 %copy-start.10 = (f32[1536]{0:T(1024)S(1)}, f32[1536]{0:T(1024)}, u32[]{:S(2)}) copy-start(f32[1536]{0:T(1024)} %param.19) | copy-start | bytes 18436
  34.4 2.7 copy-start.6
  34.4 2.7 copy-start.4
  34.4 3.4 copy-start.11
  37.9 3.8 copy-start.5
  41.6 323.6 %all-reduce.7.cloned.1.call-start = ((), (), s32[]{:S(2)}) async-start(), calls=%async_computation.3 | async-start | bytes 6291456 | tf_op jit(solution)/shard_map/psum | solution.py:90
  47.1 323.4 %all-gather.4.cloned.1.call-start = ((), (), s32[]{:S(2)}) async-start(), calls=%async_computation.2 | async-start | bytes 1966080 | tf_op jit(solution)/shard_map/all_gather | solution.py:85
  72.6 298.0 %all-gather.6.cloned.1.call-start = ((), (), s32[]{:S(2)}) async-start(), calls=%async_computation.4 | async-start | bytes 15728640 | tf_op jit(solution)/shard_map/all_gather | solution.py:89
  391.8 26.6 %copy-start.1 = (bf16[1024,1536]{1,0:T(8,128)(2,1)S(1)}, bf16[1024,1536]{1,0:T(8,128)(2,1)}, u32[]{:S(2)}) copy-start(bf16[1024,1536]{1,0:T(8,128)(2,1)} %param.14) | copy-start | bytes 9437188
Sparse Core Ops, SparseCore 0:
  41.7 30.7 reduce-scatter.1
  74.1 19.8 all-gather.3
  96.1 252.3 all-gather.5
Sparse Core Ops, SparseCore 1:
  47.2 317.9 all-reduce.6
